TPU v7x, 128 devices: a whole 4x4x4 slice. The times are simulated.
128 devices in a mesh: rep: 2 (over z_hi), fs: 32 (over z_lo, y, x), tp: 2 (over core).
Axes of the slice: x: 4, y: 4, z: 4 (z_hi: 2, z_lo: 2; z = z_hi * 2 + z_lo), core: 2. Of those that a mesh axis runs over, the one named last changes fastest.
Arguments:
- tokens: bfloat16 [65536, 2048], P(('rep', 'fs')), may hold values from -6 to 6
- norm_mix: bfloat16 [2048], replicated, may hold values from 0.099609375 to 1.8984375
- w_unit: bfloat16 [2048, 1024], P('fs', 'tp'), may hold values from -0.125 to 0.125
- w_value: bfloat16 [2048, 1024], P('fs', 'tp'), may hold values from -0.125 to 0.125
- spatial: bfloat16 [4, 128, 128], replicated, may hold values from -0.52734375 to 0.52734375
- spatial_bias: bfloat16 [4, 128], replicated, may hold values from 0.099609375 to 1.8984375
- group_gain: bfloat16 [1024], replicated, may hold values from 0.099609375 to 1.8984375
- group_shift: bfloat16 [1024], replicated, may hold values from -3 to 3
- w_mix_out: bfloat16 [1024, 2048], P('tp', 'fs'), may hold values from -0.1875 to 0.1875
- norm_ffn: bfloat16 [2048], replicated, may hold values from 0.099609375 to 1.8984375
- w_gate: bfloat16 [2048, 2816], P('fs', 'tp'), may hold values from -0.125 to 0.125
- w_up: bfloat16 [2048, 2816], P('fs', 'tp'), may hold values from -0.125 to 0.125
- w_down: bfloat16 [2816, 2048], P('tp', 'fs'), may hold values from -0.109375 to 0.109375
Outputs:
- layer_out: bfloat16 [65536, 2048], P(('rep', 'fs', 'tp'))
All inputs are finite; a program needn't handle non-finite values.
Results may differ from a plain program's by a relative error of at most 0.008.
Values may be sent and summed in bfloat16 or wider, within the bound.
No kernel may reach another device: no remote copies, remote signals or barrier semaphores. Data moves between devices by JAX's collectives and lax.ppermute only.
A program may use at most 128 MiB of HBM per device.

v0:
```python
import jax
import jax.numpy as jnp
from jax import lax
from jax.sharding import PartitionSpec as P


def sent_together(arrays, axis, dim, along):
    ends, at = ([], 0)
    for a in arrays[:-1]:
        at += a.shape[along]
        ends.append(at)
    both = jnp.concatenate(arrays, axis=along)
    return tuple(jnp.split(lax.all_gather(both, axis, axis=dim, tiled=True), ends, axis=along))


def sent_to_all(x, axis):
    copies = jnp.broadcast_to(x, (lax.axis_size(axis), *x.shape))
    return lax.all_to_all(copies, axis, split_axis=0, concat_axis=0, tiled=True)


def in_order(pieces, dim):
    pieces = jnp.moveaxis(pieces, 0, dim)
    dims = pieces.shape
    return pieces.reshape(*dims[:dim], dims[dim] * dims[dim + 1], *dims[dim + 2 :])


def gathered_copies(x, axis, dim):
    pieces = sent_to_all(x, axis)
    return in_order(pieces, dim)


def total_of_pieces(x, axis):
    return lax.all_gather(x, axis).sum(0)


def split_up(x, dim, peers):
    before, after = (x.shape[:dim], x.shape[dim + 1 :])
    return jnp.moveaxis(x.reshape(*before, peers, -1, *after), dim, 0)


def summed_on_arrival(x, axis, dim):
    pieces = split_up(x, dim, lax.axis_size(axis))
    arrived = lax.all_to_all(pieces, axis, split_axis=0, concat_axis=0, tiled=True)
    return arrived.astype(jnp.float32).sum(axis=0)


def rms_scale(values, gain):
    values = values.astype(jnp.float32)
    scale = lax.rsqrt(jnp.mean(values * values, axis=-1, keepdims=True) + 1e-06)
    return values * scale * gain.astype(jnp.float32)


def spatial_unit(unit_pre, value_pre, spatial, spatial_bias, group_gain, group_shift):
    count, width = value_pre.shape
    groups = spatial.shape[0]
    block = spatial.shape[1]
    active = jax.nn.gelu(value_pre, approximate=True).reshape(count, groups, width // groups)
    center = jnp.mean(active, axis=-1, keepdims=True)
    spread = jnp.mean(jnp.square(active - center), axis=-1, keepdims=True)
    normal = ((active - center) * lax.rsqrt(spread + 1e-06)).reshape(count, width)
    normal = normal * group_gain.astype(jnp.float32) + group_shift.astype(jnp.float32)
    grouped = normal.astype(jnp.bfloat16)
    causal = jnp.tril(jnp.ones((block, block), dtype=bool))
    weights = jnp.where(causal[None], spatial, jnp.zeros_like(spatial))
    tiles = grouped.reshape(count // block, block, groups, width // groups)
    mixed = jnp.einsum("gts,nsgd->ntgd", weights, tiles, preferred_element_type=jnp.float32)
    mixed = mixed + spatial_bias.astype(jnp.float32).T[None, :, :, None]
    return jax.nn.gelu(unit_pre, approximate=True) * mixed.reshape(count, width)


def on_device(
    tokens,
    norm_mix,
    w_unit,
    w_value,
    spatial,
    spatial_bias,
    group_gain,
    group_shift,
    w_mix_out,
    norm_ffn,
    w_gate,
    w_up,
    w_down,
):
    count = tokens.shape[0]
    half = count // lax.axis_size("tp")
    position = lax.axis_index("tp")
    row_start = position * half
    local_width = w_unit.shape[1]
    group_count = spatial.shape[0] // lax.axis_size("tp")
    group_start = position * group_count
    spatial_local = lax.dynamic_slice_in_dim(spatial, group_start, group_count, 0)
    bias_local = lax.dynamic_slice_in_dim(spatial_bias, group_start, group_count, 0)
    gain_local = lax.dynamic_slice_in_dim(group_gain, position * local_width, local_width, 0)
    shift_local = lax.dynamic_slice_in_dim(group_shift, position * local_width, local_width, 0)
    normed = rms_scale(tokens, norm_mix).astype(jnp.bfloat16)
    unit_whole, value_whole = sent_together((w_unit, w_value), "fs", 0, 1)
    unit_pre = jnp.dot(normed, unit_whole, preferred_element_type=jnp.float32)
    value_pre = jnp.dot(normed, value_whole, preferred_element_type=jnp.float32)
    gated = spatial_unit(
        unit_pre, value_pre, spatial_local, bias_local, gain_local, shift_local
    ).astype(jnp.bfloat16)
    partial_terms = jnp.dot(
        gated, gathered_copies(w_mix_out, "fs", 1), preferred_element_type=jnp.float32
    )
    summed = total_of_pieces(partial_terms, "tp")
    h_mid = (tokens.astype(jnp.float32) + summed).astype(jnp.bfloat16)
    normed_mid = rms_scale(h_mid, norm_ffn).astype(jnp.bfloat16)
    gate_whole, up_whole = sent_together((w_gate, w_up), "fs", 0, 1)
    gate = jnp.dot(normed_mid, gate_whole, preferred_element_type=jnp.float32)
    up = jnp.dot(normed_mid, up_whole, preferred_element_type=jnp.float32)
    hidden = (jax.nn.silu(gate) * up).astype(jnp.bfloat16)
    down_cols = lax.all_gather(w_down, "fs", axis=1, tiled=True)
    residual_rows = lax.dynamic_slice_in_dim(h_mid, row_start, half, 0).astype(jnp.float32)
    summed_rows = summed_on_arrival(
        jnp.dot(hidden, down_cols, preferred_element_type=jnp.float32).astype(jnp.bfloat16), "tp", 0
    )
    return (residual_rows + summed_rows).astype(jnp.bfloat16)


def solution(mesh):
    placed = (
        P(("rep", "fs"), None),
        P(),
        P("fs", "tp"),
        P("fs", "tp"),
        P(),
        P(),
        P(),
        P(),
        P("tp", "fs"),
        P(),
        P("fs", "tp"),
        P("fs", "tp"),
        P("tp", "fs"),
    )
    return jax.shard_map(
        on_device,
        mesh=mesh,
        in_specs=placed,
        out_specs=P(("rep", "fs", "tp"), None),
        check_vma=False,
    )
```

profile of v0, /device:TPU:1, one launch (start us, length us, event | category | flops | bytes accessed | tf_op | source)
XLA Modules:
  0.0 629.2 jit_solution(16438548954573870074)
XLA Ops:
  6.6 1.6 pad_maximum_fusion.1
  8.2 2.4 broadcast_in_dim.13
  10.6 9.3 %all-to-all-start = ((bf16[32,512,64]{1,2,0:T(8,128)(2,1)}), bf16[32,512,64]{1,2,0:T(8,128)(2,1)}, u32[]{:S(2)}, u32[]{:S(2)}) async-start(bf16[32,512,64]{1,2,0:T(8,128)(2,1)} %broadcast_in_dim.13), calls=%async_computation | async-start | bytes 4194304 | tf_op jit(solution)/shard_map/all_to_all | solution.py:18
  20.1 3.1 fusion.3
  23.3 133.9 %all-gather.6.cloned.1.call-done = bf16[2048,1024]{1,0:T(8,128)(2,1)} async-done(((bf16[64,1024]{1,0:T(8,128)(2,1)}), bf16[2048,1024]{1,0:T(8,128)(2,1)}) %all-gather.6.cloned.1.call-update) | async-done | bytes 4194320 | tf_op jit(solution)/shard_map/all_gather | solution.py:13
  157.1 6.9 %fusion.35 = f32[1024,512]{1,0:T(8,128)} fusion(bf16[2048,1024]{1,0:T(8,128)(2,1)} %all-gather.6.cloned.1.call-done, bf16[1024,2048]{1,0:T(8,128)(2,1)} %param.13, f32[2048]{0:T(1024)S(1)} %convert_element_type.51, f32[1024]{0:T(1024)S(1)} %add_rsqrt_fusion.2), kind=kOutput, calls=%fused_computation.39 | convolution fusion | flops 2160066560 | bytes 8400896 | tf_op jit(solution)/shard_map/dot_general | solution.py:100
  164.1 2.6 reshape.58
  166.7 1.2 reduce_sum.55
  167.9 14.4 %multiply_reduce_fusion = f32[1024,2]{1,0:T(8,128)S(1)} fusion(f32[1024,2,256]{2,1,0:T(2,128)S(1)} %reshape.58, f32[1024,2]{1,0:T(8,128)S(1)} %broadcast_multiply_fusion), kind=kLoop, calls=%fused_computation.46 | loop fusion | flops 1570816 | bytes 2113536 | tf_op jit(solution)/shard_map/reduce_sum | solution.py:59
  182.4 1.2 mul.112
  183.6 0.2 copy.32
  183.8 1.2 sub.17
  185.4 0.8 add_convert_fusion.1
  186.2 0.3 reshape.59
  186.5 0.5 bitcast_add_fusion
  187.1 2.4 copy.28
  189.5 1.8 copy.33
  191.3 11.6 %fusion.51 = f32[1024,2048]{1,0:T(8,128)} fusion(bf16[512,2048]{0,1:T(8,128)(2,1)} %bitcast.5, f32[1024,512]{1,0:T(8,128)S(1)} %bitcast.30, bf16[2048,1024]{1,0:T(8,128)(2,1)} %all-gather.6.cloned.1.call-done, bf16[1024,2048]{1,0:T(8,128)(2,1)} %param.13, f32[2048]{0:T(1024)S(1)} %convert_element_type.51, f32[1024]{0:T(1024)S(1)} %add_rsqrt_fusion.2), kind=kOutput, calls=%fused_computation.47 | convolution fusion | flops 4308598784 | bytes 18886656 | tf_op jit(solution)/shard_map/dot_general | solution.py:104
  203.0 0.8 copy-done.2
  203.9 0.8 pad_maximum_fusion
  204.7 0.5 all-gather.10.cloned.1.call-update
  205.3 49.1 %all-gather.12.cloned.1.call-done = f32[2048,2048]{1,0:T(8,128)} async-done(((f32[1024,2048]{1,0:T(8,128)}), f32[2048,2048]{1,0:T(8,128)}) %all-gather.12.cloned.1.call-update) | async-done | bytes 16777232 | tf_op jit(solution)/shard_map/all_gather | solution.py:33
  254.4 11.8 %reduce_sum.57 = f32[1024,2048]{1,0:T(8,128)} reduce(f32[2,1024,2048]{2,1,0:T(8,128)} %bitcast.23, f32[]{:T(128)} %constant.15.clone.1), dimensions={0}, to_apply=%region_3.4 | reduce | flops 2097152 | bytes 25165828 | tf_op jit(solution)/shard_map/reduce_sum | solution.py:33
  266.1 7.8 %fusion = (f32[1024]{0:T(1024)S(1)}, bf16[1024,2048]{1,0:T(8,128)(2,1)}) fusion(f32[1024,2048]{1,0:T(8,128)} %reduce_sum.57, bf16[1024,2048]{1,0:T(8,128)(2,1)} %param.13), kind=kLoop, calls=%fused_computation.5 | loop fusion | flops 12581888 | bytes 16781312 | tf_op jit(solution)/shard_map/reduce_sum | solution.py:49
  273.9 135.7 %all-gather.8.cloned.1.call-done = bf16[2048,2816]{1,0:T(8,128)(2,1)} async-done(((bf16[64,2816]{1,0:T(8,128)(2,1)}), bf16[2048,2816]{1,0:T(8,128)(2,1)}) %all-gather.8.cloned.1.call-update) | async-done | bytes 11534352 | tf_op jit(solution)/shard_map/all_gather | solution.py:13
  409.6 11.9 %fusion.9 = f32[1024,1408]{1,0:T(8,128)} fusion(bf16[2048,2816]{1,0:T(8,128)(2,1)} %all-gather.8.cloned.1.call-done, bf16[1024,2048]{1,0:T(8,128)(2,1)} %get-tuple-element.6, f32[2048]{0:T(1024)S(1)} %convert_element_type.60, f32[1024]{0:T(1024)S(1)} %add_rsqrt_fusion.1), kind=kOutput, calls=%fused_computation.15 | convolution fusion | flops 5913968640 | bytes 15740928 | tf_op jit(solution)/shard_map/dot_general | solution.py:111
  421.5 147.9 %all-gather.10.cloned.1.call-done = bf16[1408,2048]{0,1:T(8,128)(2,1)} async-done(((bf16[1408,64]{0,1:T(8,128)(2,1)}), bf16[1408,2048]{0,1:T(8,128)(2,1)}) %all-gather.10.cloned.1.call-update) | async-done | bytes 5767184 | tf_op jit(solution)/shard_map/all_gather | solution.py:114
  569.4 20.9 %fusion.16 = bf16[1024,2048]{1,0:T(8,128)(2,1)} fusion(bf16[1408,2048]{0,1:T(8,128)(2,1)} %all-gather.10.cloned.1.call-done, f32[1024,1408]{1,0:T(8,128)} %fusion.9, bf16[2048,2816]{1,0:T(8,128)(2,1)} %all-gather.8.cloned.1.call-done, bf16[1024,2048]{1,0:T(8,128)(2,1)} %get-tuple-element.6, f32[2048]{0:T(1024)S(1)} %convert_element_type.60, ...), kind=kOutput, calls=%fused_computation.20 | convolution fusion | flops 11830296576 | bytes 25702400 | tf_op jit(solution)/shard_map/dot_general | solution.py:117
  590.3 28.2 %all_to_all.10 = bf16[2,512,2048]{2,1,0:T(8,128)(2,1)S(1)} all-to-all(bf16[2,512,2048]{2,1,0:T(8,128)(2,1)} %bitcast.29), channel_id=1, replica_groups=mesh['rep'=2,'fs'=32,'tp'=2] {'tp'}, dimensions={0} | all-to-all | bytes 8388608 | tf_op jit(solution)/shard_map/all_to_all | solution.py:43
  618.5 1.0 convert_reduce_fusion
  619.4 1.2 copy-done
  620.7 2.1 add_convert_fusion
  (36 shorter events, 0.9 us)
Async XLA Ops:
  6.5 13.4 %copy-start.5 = (bf16[2048]{0:T(1024)(128)(2,1)S(1)}, bf16[2048]{0:T(1024)(128)(2,1)}, u32[]{:S(2)}) copy-start(bf16[2048]{0:T(1024)(128)(2,1)} %param.14) | copy-start | bytes 12292
  6.5 13.5 %copy-start.9 = (bf16[4,128]{1,0:T(4,128)(2,1)S(1)}, bf16[4,128]{1,0:T(4,128)(2,1)}, u32[]{:S(2)}) copy-start(bf16[4,128]{1,0:T(4,128)(2,1)} %param.18) | copy-start | bytes 3076
  6.5 13.5 %copy-start.8 = (bf16[1024]{0:T(1024)(128)(2,1)S(1)}, bf16[1024]{0:T(1024)(128)(2,1)}, u32[]{:S(2)}) copy-start(bf16[1024]{0:T(1024)(128)(2,1)} %param.19) | copy-start | bytes 6148
  6.5 13.5 %copy-start.7 = (bf16[1024]{0:T(1024)(128)(2,1)S(1)}, bf16[1024]{0:T(1024)(128)(2,1)}, u32[]{:S(2)}) copy-start(bf16[1024]{0:T(1024)(128)(2,1)} %param.20) | copy-start | bytes 6148
  6.5 150.6 %all-gather.6.cloned.1.call-start = ((), (), s32[]{:S(2)}) async-start(), calls=%async_computation.2 | async-start | bytes 4325376 | tf_op jit(solution)/shard_map/all_gather | solution.py:13
  10.6 180.7 %all-to-all-start = ((bf16[32,512,64]{1,2,0:T(8,128)(2,1)}), bf16[32,512,64]{1,2,0:T(8,128)(2,1)}, u32[]{:S(2)}, u32[]{:S(2)}) async-start(bf16[32,512,64]{1,2,0:T(8,128)(2,1)} %broadcast_in_dim.13), calls=%async_computation | async-start | bytes 4194304 | tf_op jit(solution)/shard_map/all_to_all | solution.py:18
  19.9 234.4 %all-gather.12.cloned.1.call-start = ((), (), s32[]{:S(2)}) async-start(), calls=%async_computation.5 | async-start | bytes 25165824 | tf_op jit(solution)/shard_map/all_gather | solution.py:33
  183.8 1.6 copy-start.1
  185.4 1.1 copy-start.4
  202.9 0.9 copy-start.2
  202.9 1.0 copy-start.3
  202.9 2.4 copy-start.6
  202.9 206.7 %all-gather.8.cloned.1.call-start = ((), (), s32[]{:S(2)}) async-start(), calls=%async_computation.3 | async-start | bytes 11894784 | tf_op jit(solution)/shard_map/all_gather | solution.py:13
  204.7 364.7 %all-gather.10.cloned.1.call-start = ((), (), s32[]{:S(2)}) async-start(), calls=%async_computation.4 | async-start | bytes 5947392 | tf_op jit(solution)/shard_map/all_gather | solution.py:114
  618.5 2.2 copy-start
Sparse Core Ops, SparseCore 0:
  9.0 148.1 all-gather.5
  203.0 51.2 all-gather.11
  256.0 153.5 all-gather.7
  411.1 158.2 all-gather.9
where the time goes:
time: 630 us; the launch traced here: 629 us
  waiting for transfers between devices  467 us (74%)
  matrix products  51.8 us (8%)
  other arithmetic  44.6 us (7%)
  blocking collectives  28.2 us (4%)
  local copies, waits for them, and re-layouts  14.5 us (2%)
  between operations  13.3 us (2%)
  starting transfers between devices  9.5 us (2%)
    all_gather x2, waiting for transfers between devices, sent_together(): lax.all_gather(both, axis, axis=dim, tiled=True)  270 us
    all_gather x1, waiting for transfers between devices, on_device(): down_cols = lax.all_gather(w_down, 'fs', axis=1, tiled=True)  148 us
    all_gather x1, waiting for transfers between devices, total_of_pieces(): return lax.all_gather(x, axis).sum(0)  49.1 us
    all_to_all x1, blocking collectives, summed_on_arrival(): lax.all_to_all(pieces, axis, split_axis=0, concat_axis=0, tiled=True)  28.2 us
    dot_general x1, matrix products, on_device(): jnp.dot(hidden, down_cols, preferred_element_type=jnp.float32)  20.9 us
    reduce_sum x1, other arithmetic, spatial_unit(): spread = jnp.mean(jnp.square(active - center), axis=-1, keepdims=True)  14.4 us
  transfers between devices with their start and end apart: 5, of which 4 were waited for; matrix products, arithmetic and copies ran while one was open for 11% of the time, Pallas kernels for 0%

commit v1 on v0

v1 whole, which is shorter than its diff:
```python
import jax
import jax.numpy as jnp
from jax import lax
from jax.sharding import PartitionSpec as P

EVERY = ("tp", "rep", "fs")


def rms_scale(values, gain):
    values = values.astype(jnp.float32)
    scale = lax.rsqrt(jnp.mean(values * values, axis=-1, keepdims=True) + 1e-06)
    return values * scale * gain.astype(jnp.float32)


def spatial_unit(unit_pre, value_pre, spatial, spatial_bias, group_gain, group_shift):
    count, width = value_pre.shape
    groups = spatial.shape[0]
    block = spatial.shape[1]
    active = jax.nn.gelu(value_pre, approximate=True).reshape(count, groups, width // groups)
    center = jnp.mean(active, axis=-1, keepdims=True)
    spread = jnp.mean(jnp.square(active - center), axis=-1, keepdims=True)
    normal = ((active - center) * lax.rsqrt(spread + 1e-06)).reshape(count, width)
    normal = normal * group_gain.astype(jnp.float32) + group_shift.astype(jnp.float32)
    grouped = normal.astype(jnp.bfloat16)
    causal = jnp.tril(jnp.ones((block, block), dtype=bool))
    weights = jnp.where(causal[None], spatial, jnp.zeros_like(spatial))
    tiles = grouped.reshape(count // block, block, groups, width // groups)
    mixed = jnp.einsum("gts,nsgd->ntgd", weights, tiles, preferred_element_type=jnp.float32)
    mixed = mixed + spatial_bias.astype(jnp.float32).T[None, :, :, None]
    return jax.nn.gelu(unit_pre, approximate=True) * mixed.reshape(count, width)


def dot_nt(a, b):
    return lax.dot_general(a, b, (((1,), (1,)), ((), ())), preferred_element_type=jnp.float32)


def dot_nn(a, b):
    return jnp.dot(a, b, preferred_element_type=jnp.float32)


def half_rows(x, part):
    size = x.shape[0] // 2
    return lax.dynamic_slice_in_dim(x, part * size, size, 0)


def in_rows(x):
    rep, fs, rows, k = x.shape
    return x.transpose(1, 0, 2, 3).reshape(fs * rep * rows, k)


def on_device(
    tokens, norm_mix, w_unit, w_value, spatial, spatial_bias, group_gain, group_shift,
    w_mix_out, norm_ffn, w_gate, w_up, w_down,
):
    rep = lax.axis_index("rep")
    reps, fs, tps = (lax.axis_size(a) for a in ("rep", "fs", "tp"))
    rows = tokens.shape[0] // tps
    mine = lax.dynamic_slice_in_dim(tokens, lax.axis_index("tp") * rows, rows, 0)

    first = jnp.concatenate(
        [jnp.where(rep == 0, w_unit, w_value), half_rows(w_mix_out.T, rep)], axis=0
    )
    second = jnp.concatenate(
        [jnp.where(rep == 0, w_gate, w_up), half_rows(w_down.T, rep)], axis=0
    )
    share = w_unit.shape[0]
    one = lax.all_gather(first, EVERY).reshape(tps, reps, fs, *first.shape)
    two = lax.all_gather(second, EVERY).reshape(tps, reps, fs, *second.shape)
    pre = one[:, :, :, :share].reshape(tps, reps, fs * share, -1)
    mid = two[:, :, :, :share].reshape(tps, reps, fs * share, -1)

    normed = rms_scale(mine, norm_mix).astype(jnp.bfloat16)
    unit_pre = jnp.concatenate([dot_nn(normed, pre[t, 0]) for t in range(tps)], axis=1)
    value_pre = jnp.concatenate([dot_nn(normed, pre[t, 1]) for t in range(tps)], axis=1)
    gated = spatial_unit(
        unit_pre, value_pre, spatial, spatial_bias, group_gain, group_shift
    ).astype(jnp.bfloat16)
    out_w = jnp.concatenate([in_rows(one[t, :, :, share:]) for t in range(tps)], axis=1)
    h_mid = (mine.astype(jnp.float32) + dot_nt(gated, out_w)).astype(jnp.bfloat16)
    normed_mid = rms_scale(h_mid, norm_ffn).astype(jnp.bfloat16)
    hidden = jnp.concatenate(
        [
            (jax.nn.silu(dot_nn(normed_mid, mid[t, 0])) * dot_nn(normed_mid, mid[t, 1])).astype(jnp.bfloat16)
            for t in range(tps)
        ],
        axis=1,
    )
    down = jnp.concatenate([in_rows(two[t, :, :, share:]) for t in range(tps)], axis=1)
    return (h_mid.astype(jnp.float32) + dot_nt(hidden, down)).astype(jnp.bfloat16)


def solution(mesh):
    placed = (
        P(("rep", "fs"), None), P(), P("fs", "tp"), P("fs", "tp"), P(), P(), P(), P(),
        P("tp", "fs"), P(), P("fs", "tp"), P("fs", "tp"), P("tp", "fs"),
    )
    return jax.shard_map(
        on_device, mesh=mesh, in_specs=placed, out_specs=P(("rep", "fs", "tp"), None), check_vma=False
    )
```

time: 630 us -> 269 us (0.43)
  waiting for transfers between devices: 467 us -> 150 us
  other arithmetic: 44.6 us -> 6.87 us
  local copies, waits for them, and re-layouts: 14.5 us -> 48.5 us
  blocking collectives: 28.2 us -> 0 us
  starting transfers between devices: 9.5 us -> 0.08 us
    all_gather x4 -> x2, waiting for transfers between devices: 467 us -> 150 us  [the longest x1 75.7 us: on_device(): two = lax.all_gather(second, EVERY).reshape(tps, reps, fs, *second.shape)]
    all_to_all x1 -> x0, blocking collectives: 28.2 us -> none  [summed_on_arrival(): lax.all_to_all(pieces, axis, split_axis=0, concat_axis=0, tiled=True)]
    slice x0 -> x2, local copies, waits for them, and re-layouts: none -> 20.7 us  [the longest x1 12.9 us: on_device(): mid = two[:, :, :, :share].reshape(tps, reps, fs * share, -1)]
    transpose x0 -> x6, local copies, waits for them, and re-layouts: none -> 16.8 us  [in_rows(): return x.transpose(1, 0, 2, 3).reshape(fs * rep * rows, k)]
    reduce_sum x1, other arithmetic: 14.4 us -> 0.83 us  [spatial_unit(): spread = jnp.mean(jnp.square(active - center), axis=-1, keepdims=True)]
    reduce_sum x2 -> x0, other arithmetic: 12.7 us -> none  [the longest x1 11.8 us: total_of_pieces(): return lax.all_gather(x, axis).sum(0)]
    all_to_all x1 -> x0, starting transfers between devices: 9.34 us -> none  [sent_to_all(): return lax.all_to_all(copies, axis, split_axis=0, concat_axis=0, tiled=True)]
    reduce_sum x2 -> x1, other arithmetic: 10.9 us -> 2.08 us  [rms_scale(): scale = lax.rsqrt(jnp.mean(values * values, axis=-1, keepdims=True) + 1e-06)]
  transfers between devices with their start and end apart: 5 -> 2, of which waited for: 4 -> 2; matrix products, arithmetic and copies ran while one was open for 11% -> 13% of each run, Pallas kernels for 0% -> 0%
where the time goes in v1:
time: 269 us
  waiting for transfers between devices  150 us (56%)
  matrix products  49.6 us (18%)
  local copies, waits for them, and re-layouts  48.5 us (18%)
  between operations  13.8 us (5%)
  other arithmetic  6.87 us (3%)
    all_gather x1, waiting for transfers between devices, on_device(): two = lax.all_gather(second, EVERY).reshape(tps, reps, fs, *second.shape)  75.7 us
    all_gather x1, waiting for transfers between devices, on_device(): one = lax.all_gather(first, EVERY).reshape(tps, reps, fs, *first.shape)  74.1 us
    dot_general x8, matrix products, dot_nn(): return jnp.dot(a, b, preferred_element_type=jnp.float32)  36.4 us
    transpose x6, local copies, waits for them, and re-layouts, in_rows(): return x.transpose(1, 0, 2, 3).reshape(fs * rep * rows, k)  16.8 us
    slice x1, local copies, waits for them, and re-layouts, on_device(): mid = two[:, :, :, :share].reshape(tps, reps, fs * share, -1)  12.9 us
    dot_general x2, matrix products, dot_nt(): lax.dot_general(a, b, (((1,), (1,)), ((), ())), preferred_element_type=jn...  12 us
    slice x1, local copies, waits for them, and re-layouts, on_device(): pre = one[:, :, :, :share].reshape(tps, reps, fs * share, -1)  7.8 us
    unnamed x43, local copies, waits for them, and re-layouts  7 us
  transfers between devices with their start and end apart: 2, of which 2 were waited for; matrix products, arithmetic and copies ran while one was open for 13% of the time, Pallas kernels for 0%

profile of v1, /device:TPU:1, one launch (start us, length us, event | category | flops | bytes accessed | tf_op | source)
XLA Modules:
  0.0 268.7 jit_solution(9162403091080069551)
XLA Ops:
  6.6 0.8 dynamic-slice_bitcast_fusion.1
  7.4 0.9 broadcast_select_fusion.1
  9.1 1.0 broadcast_select_fusion
  10.0 0.7 pad_maximum_fusion
  10.9 2.1 fusion.8
  13.0 74.1 %all-gather.5.cloned.1.call-done = bf16[12288,512]{1,0:T(8,128)(2,1)} async-done(((bf16[96,512]{1,0:T(8,128)(2,1)}), bf16[12288,512]{1,0:T(8,128)(2,1)}) %all-gather.5.cloned.1.call-update) | async-done | bytes 12582928 | tf_op jit(solution)/shard_map/all_gather | solution.py:67
  87.1 7.8 %slice.56 = bf16[2,2,32,64,512]{4,3,2,1,0:T(8,128)(2,1)} slice(bf16[2,2,32,96,512]{4,3,2,1,0:T(8,128)(2,1)} %bitcast.98), slice={[0:2], [0:2], [0:32], [0:64], [0:512]} | slice | bytes 16777216 | tf_op jit(solution)/shard_map/slice | solution.py:69
  94.9 3.6 %fusion.59 = f32[512,512]{0,1:T(8,128)S(1)} fusion(bf16[2,2,2048,512]{3,2,1,0:T(8,128)(2,1)} %bitcast.104, f32[2048]{0:T(1024)S(1)} %convert_element_type.43, f32[512]{0:T(512)S(1)} %add_rsqrt_fusion.2, bf16[1024,2048]{1,0:T(8,128)(2,1)} %param.13, s32[]{:T(128)S(6)} %select_n.29), kind=kOutput, calls=%fused_computation.74 | convolution fusion | flops 1077936128 | bytes 5253124 | tf_op jit(solution)/shard_map/dot_general | solution.py:38
  98.9 3.8 %fusion.58 = f32[512,512]{0,1:T(8,128)S(1)} fusion(bf16[2,2,2048,512]{3,2,1,0:T(8,128)(2,1)} %bitcast.105, f32[2048]{0:T(1024)S(1)} %convert_element_type.43, f32[512]{0:T(512)S(1)} %add_rsqrt_fusion.2, bf16[1024,2048]{1,0:T(8,128)(2,1)} %param.13, s32[]{:T(128)S(6)} %select_n.29), kind=kOutput, calls=%fused_computation.72 | convolution fusion | flops 1077936128 | bytes 5253124 | tf_op jit(solution)/shard_map/dot_general | solution.py:38
  102.7 1.3 concatenate.36
  104.0 0.7 fusion.76
  104.7 0.8 multiply_reduce_fusion
  105.7 1.1 copy-done.3
  106.9 1.2 bitcast_add_fusion
  108.1 1.4 copy.22
  109.5 2.7 %slice_bitcast_fusion.19 = (bf16[32,2,32,512]{3,2,0,1:T(8,128)(2,1)S(1)}, bf16[32,2,32,512]{3,2,0,1:T(8,128)(2,1)S(1)}) fusion(bf16[2,2,32,96,512]{4,3,2,1,0:T(8,128)(2,1)} %bitcast.99), kind=kLoop, calls=%fused_computation.70 | loop fusion | bytes 8388608 | tf_op jit(solution)/shard_map/transpose | solution.py:48
  112.9 1.6 slice-done.5
  114.5 1.1 copy-done.4
  115.7 1.4 fusion.60
  117.2 1.6 fusion.61
  118.8 2.8 %fusion.12 = (f32[512]{0:T(512)S(1)}, bf16[512,2048]{1,0:T(8,128)(2,1)S(1)}) fusion(bf16[2048,512]{1,0:T(8,128)(2,1)S(1)} %bitcast.114, bf16[2048,512]{1,0:T(8,128)(2,1)S(1)} %bitcast.113, f32[128,8,4,128]{3,2,1,0:T(4,128)S(1)} %bitcast.112, f32[512,512]{0,1:T(8,128)S(1)} %fusion.60, f32[512,512]{0,1:T(8,128)S(1)} %fusion.61, ...), kind=kOutput, calls=%fused_computation.24 | convolution fusion | flops 2167930368 | bytes 12584964 | tf_op jit(solution)/shard_map/dot_general | solution.py:34
  121.6 75.7 %all-gather.7.cloned.1.call-done = bf16[12288,1408]{1,0:T(8,128)(2,1)} async-done(((bf16[96,1408]{1,0:T(8,128)(2,1)}), bf16[12288,1408]{1,0:T(8,128)(2,1)}) %all-gather.7.cloned.1.call-update) | async-done | bytes 34603024 | tf_op jit(solution)/shard_map/all_gather | solution.py:68
  197.4 12.9 %slice.63 = bf16[2,2,32,64,1408]{4,3,2,1,0:T(8,128)(2,1)S(1)} slice(bf16[2,2,32,96,1408]{4,3,2,1,0:T(8,128)(2,1)} %bitcast.88), slice={[0:2], [0:2], [0:32], [0:64], [0:1408]} | slice | bytes 46137344 | tf_op jit(solution)/shard_map/slice | solution.py:70
  210.3 5.7 %fusion.7 = f32[512,1408]{1,0:T(8,128)} fusion(bf16[2,2,2048,1408]{3,2,1,0:T(8,128)(2,1)S(1)} %bitcast.90, bf16[512,2048]{1,0:T(8,128)(2,1)S(1)} %get-tuple-element.10, f32[2048]{0:T(1024)S(1)} %convert_element_type.49, f32[512]{0:T(512)S(1)} %add_rsqrt_fusion.1), kind=kOutput, calls=%fused_computation.19 | convolution fusion | flops 2956984320 | bytes 10758144 | tf_op jit(solution)/shard_map/dot_general | solution.py:38
  216.0 2.7 %copy-done.2 = bf16[2,2,32,64,1408]{4,3,2,1,0:T(8,128)(2,1)} copy-done((bf16[2,2,32,64,1408]{4,3,2,1,0:T(8,128)(2,1)}, bf16[2,2,32,64,1408]{4,3,2,1,0:T(8,128)(2,1)S(1)}, u32[]{:S(2)}) %copy-start.2) | copy-done | bytes 23068696
  218.7 5.0 %fusion.5 = f32[512,1408]{1,0:T(8,128)S(1)} fusion(bf16[2,2,2048,1408]{3,2,1,0:T(8,128)(2,1)S(1)} %bitcast.91, bf16[512,2048]{1,0:T(8,128)(2,1)} %copy-done.11, f32[2048]{0:T(1024)S(1)} %convert_element_type.49, f32[512]{0:T(512)S(1)} %add_rsqrt_fusion.1), kind=kOutput, calls=%fused_computation.15 | convolution fusion | flops 2956984320 | bytes 10758144 | tf_op jit(solution)/shard_map/dot_general | solution.py:38
  223.8 9.5 %slice_bitcast_fusion.1 = (bf16[32,2,32,1408]{3,2,0,1:T(8,128)(2,1)}, bf16[32,2,32,1408]{3,2,0,1:T(8,128)(2,1)}) fusion(bf16[2,2,32,96,1408]{4,3,2,1,0:T(8,128)(2,1)} %bitcast.89), kind=kLoop, calls=%fused_computation.11 | loop fusion | bytes 23068672 | tf_op jit(solution)/shard_map/transpose | solution.py:48
  233.3 7.7 %fusion.25 = bf16[512,1408]{1,0:T(8,128)(2,1)S(1)} fusion(bf16[2,2,2048,1408]{3,2,1,0:T(8,128)(2,1)} %bitcast.92, f32[512,1408]{1,0:T(8,128)} %fusion.7, bf16[512,2048]{1,0:T(8,128)(2,1)} %copy-done.11, f32[2048]{0:T(1024)S(1)} %convert_element_type.49, f32[512]{0:T(512)S(1)} %add_rsqrt_fusion.1), kind=kOutput, calls=%fused_computation.38 | convolution fusion | flops 2961309696 | bytes 12199936 | tf_op jit(solution)/shard_map/dot_general | solution.py:38
  241.0 7.4 %fusion.24 = bf16[512,1408]{1,0:T(8,128)(2,1)} fusion(bf16[2,2,2048,1408]{3,2,1,0:T(8,128)(2,1)} %bitcast.93, f32[512,1408]{1,0:T(8,128)S(1)} %fusion.5, bf16[512,2048]{1,0:T(8,128)(2,1)S(1)} %copy-done.12, f32[2048]{0:T(1024)S(1)} %convert_element_type.49, f32[512]{0:T(512)S(1)} %add_rsqrt_fusion.1), kind=kOutput, calls=%fused_computation.37 | convolution fusion | flops 2961309696 | bytes 12199936 | tf_op jit(solution)/shard_map/dot_general | solution.py:38
  248.5 0.9 copy.25
  249.4 3.3 %copy.26 = bf16[32,2,32,1408]{3,2,1,0:T(8,128)(2,1)} copy(bf16[32,2,32,1408]{3,2,0,1:T(8,128)(2,1)S(1)} %bitcast.95) | data formatting | bytes 11534336 | tf_op jit(solution)/shard_map/transpose | solution.py:48
  252.7 9.2 %fusion.15 = bf16[512,2048]{1,0:T(8,128)(2,1)} fusion(bf16[512,2048]{1,0:T(8,128)(2,1)S(1)} %copy-done.13, bf16[2048,1408]{1,0:T(8,128)(2,1)} %bitcast.111, bf16[2048,1408]{1,0:T(8,128)(2,1)S(1)} %bitcast.110, bf16[512,1408]{1,0:T(8,128)(2,1)S(1)} %copy-done.14, bf16[512,1408]{1,0:T(8,128)(2,1)S(1)} %fusion.25), kind=kOutput, calls=%fused_computation.27 | convolution fusion | flops 5937561600 | bytes 18612224 | tf_op jit(solution)/shard_map/dot_general | solution.py:34
  (64 shorter events, 2.2 us)
Async XLA Ops:
  6.5 2.5 copy-start
  6.5 4.3 %copy-start.5 = (bf16[2048]{0:T(1024)(128)(2,1)S(1)}, bf16[2048]{0:T(1024)(128)(2,1)}, u32[]{:S(2)}) copy-start(bf16[2048]{0:T(1024)(128)(2,1)} %param.14) | copy-start | bytes 12292
  6.5 4.3 %copy-start.7 = (bf16[1024]{0:T(1024)(128)(2,1)S(1)}, bf16[1024]{0:T(1024)(128)(2,1)}, u32[]{:S(2)}) copy-start(bf16[1024]{0:T(1024)(128)(2,1)} %param.19) | copy-start | bytes 6148
  6.5 4.3 %copy-start.8 = (bf16[1024]{0:T(1024)(128)(2,1)S(1)}, bf16[1024]{0:T(1024)(128)(2,1)}, u32[]{:S(2)}) copy-start(bf16[1024]{0:T(1024)(128)(2,1)} %param.20) | copy-start | bytes 6148
  6.5 4.3 %copy-start.6 = (bf16[2048]{0:T(1024)(128)(2,1)S(1)}, bf16[2048]{0:T(1024)(128)(2,1)}, u32[]{:S(2)}) copy-start(bf16[2048]{0:T(1024)(128)(2,1)} %param.22) | copy-start | bytes 12292
  6.5 80.6 %all-gather.5.cloned.1.call-start = ((), (), s32[]{:S(2)}) async-start(), calls=%async_computation | async-start | bytes 12681216 | tf_op jit(solution)/shard_map/all_gather | solution.py:67
  7.4 5.5 %copy-start.9 = (bf16[4,128]{1,0:T(4,128)(2,1)S(1)}, bf16[4,128]{1,0:T(4,128)(2,1)}, u32[]{:S(2)}) copy-start(bf16[4,128]{1,0:T(4,128)(2,1)} %param.18) | copy-start | bytes 3076
  9.0 188.4 %all-gather.7.cloned.1.call-start = ((), (), s32[]{:S(2)}) async-start(), calls=%async_computation.1 | async-start | bytes 34873344 | tf_op jit(solution)/shard_map/all_gather | solution.py:68
  105.6 1.2 copy-start.3
  105.6 1.3 copy-start.10
  109.4 3.5 %slice-start.4 = ((s8[8388608]{0:T(1024)(128)(4,1)}), s8[4194304]{0:T(1024)(128)(4,1)S(1)}, s32[]{:S(2)}) async-start(s8[8388608]{0:T(1024)(128)(4,1)} %bitcast.106), calls=%async_computation.6 | async-start | bytes 8388608
  112.2 2.4 slice-start.5
  112.4 3.3 %copy-start.4 = (bf16[1024,2048]{1,0:T(8,128)(2,1)S(1)}, bf16[1024,2048]{1,0:T(8,128)(2,1)}, u32[]{:S(2)}) copy-start(bf16[1024,2048]{1,0:T(8,128)(2,1)} %param.13) | copy-start | bytes 12582916
  121.6 88.7 %copy-start.11 = (bf16[512,2048]{1,0:T(8,128)(2,1)}, bf16[512,2048]{1,0:T(8,128)(2,1)S(1)}, u32[]{:S(2)}) copy-start(bf16[512,2048]{1,0:T(8,128)(2,1)S(1)} %get-tuple-element.10) | copy-start | bytes 6291460
  210.3 8.5 %copy-start.2 = (bf16[2,2,32,64,1408]{4,3,2,1,0:T(8,128)(2,1)}, bf16[2,2,32,64,1408]{4,3,2,1,0:T(8,128)(2,1)S(1)}, u32[]{:S(2)}) copy-start(bf16[2,2,32,64,1408]{4,3,2,1,0:T(8,128)(2,1)S(1)} %slice.63) | copy-start | bytes 69206016
  233.3 7.8 %copy-start.12 = (bf16[512,2048]{1,0:T(8,128)(2,1)S(1)}, bf16[512,2048]{1,0:T(8,128)(2,1)}, u32[]{:S(2)}) copy-start(bf16[512,2048]{1,0:T(8,128)(2,1)} %copy-done.11) | copy-start | bytes 6291460
  233.3 15.2 %slice-start.2 = ((s8[5767168]{0:T(1024)(128)(4,1)}), s8[4194304]{0:T(1024)(128)(4,1)S(1)}, s32[]{:S(2)}) async-start(s8[5767168]{0:T(1024)(128)(4,1)} %bitcast.96), calls=%async_computation.4 | async-start | bytes 8388608
  233.3 16.1 %slice-start = ((s8[5767168]{0:T(1024)(128)(4,1)}), s8[4194304]{0:T(1024)(128)(4,1)S(1)}, s32[]{:S(2)}) async-start(s8[5767168]{0:T(1024)(128)(4,1)} %bitcast.94), calls=%async_computation.2 | async-start | bytes 8388608
  241.0 7.5 %slice-start.3 = ((s8[5767168]{0:T(1024)(128)(4,1)}), s8[1572864]{0:T(1024)(128)(4,1)S(1)}, s32[]{:S(2)}) async-start(s8[5767168]{0:T(1024)(128)(4,1)} %bitcast.96), calls=%async_computation.5 | async-start | bytes 3145728
  241.0 8.4 %slice-start.1 = ((s8[5767168]{0:T(1024)(128)(4,1)}), s8[1572864]{0:T(1024)(128)(4,1)S(1)}, s32[]{:S(2)}) async-start(s8[5767168]{0:T(1024)(128)(4,1)} %bitcast.94), calls=%async_computation.3 | async-start | bytes 3145728
  249.4 3.3 %copy-start.13 = (bf16[512,2048]{1,0:T(8,128)(2,1)S(1)}, bf16[512,2048]{1,0:T(8,128)(2,1)}, u32[]{:S(2)}) copy-start(bf16[512,2048]{1,0:T(8,128)(2,1)} %copy-done.11) | copy-start | bytes 6291460
  249.4 3.3 %copy-start.14 = (bf16[512,1408]{1,0:T(8,128)(2,1)S(1)}, bf16[512,1408]{1,0:T(8,128)(2,1)}, u32[]{:S(2)}) copy-start(bf16[512,1408]{1,0:T(8,128)(2,1)} %fusion.24) | copy-start | bytes 4325380
  252.7 9.2 %copy-start.1 = (bf16[1408,64]{0,1:T(8,128)(2,1)S(1)}, bf16[1408,64]{0,1:T(8,128)(2,1)}, u32[]{:S(2)}) copy-start(bf16[1408,64]{0,1:T(8,128)(2,1)} %param.25) | copy-start | bytes 540676
Sparse Core Ops, SparseCore 0:
  10.5 76.6 all-gather.4
  90.1 107.1 all-gather.6
